TPU v7x, 32 devices: a whole 2x2x4 slice. The times are simulated.
32 devices in a mesh: sp: 4 (over y, x), tp: 8 (over z, core).
Axes of the slice: x: 2, y: 2, z: 4, core: 2. Of those that a mesh axis runs over, the one named last changes fastest.
Arguments:
- tokens: bfloat16 [8192, 2048], P('sp', 'tp'), may hold values from -6 to 6
- norm_gain: float32 [2048], replicated, may hold values from 0.1 to 1.9
- w_key: bfloat16 [2048, 1024], P(None, 'tp'), may hold values from -0.125 to 0.125
- w_decay: bfloat16 [2048, 1024], P(None, 'tp'), may hold values from -0.125 to 0.125
- w_value: bfloat16 [2048, 512], replicated, may hold values from -0.125 to 0.125
- decay_bias: float32 [1024], P('tp'), may hold values from 0 to 8.5
- gate_drift: float32 [8192], P('sp'), may hold values from -1 to 1
- queries: bfloat16 [1024], P('tp'), may hold values from -6 to 6
- out_gain: float32 [4, 512], P(None, 'sp'), may hold values from 0.1 to 1.9
Outputs:
- state_cache: bfloat16 [1024, 512], P('tp', 'sp')
- first_read: float32 [4, 512], P(None, 'sp')
All inputs are finite; a program needn't handle non-finite values.
Results may differ from a plain program's by a relative error of at most 0.009.
Values may be sent and summed in bfloat16 or wider, within the bound.
A program may use at most 128 MiB of HBM per device.

v0:
```python
import jax
import jax.numpy as jnp
from jax import lax
from jax.sharding import PartitionSpec as P

QUERY_KEY_HEADS = 4
KEY_CHANNELS = 256
VALUE_CHANNELS = 512
EPS = 1e-06
GATE_NORM = 16.0


def body(tokens, norm_gain, w_key, w_decay, w_value, decay_bias, gate_drift, queries, out_gain):
    gathered = lax.all_gather(tokens, "tp", axis=1, tiled=True)
    rows_f32 = gathered.astype(jnp.float32)
    inverse_rms = lax.rsqrt(jnp.mean(rows_f32 * rows_f32, axis=1, keepdims=True) + EPS)
    normed = (rows_f32 * inverse_rms * norm_gain[None, :]).astype(jnp.bfloat16)
    key_proj = jnp.dot(normed, w_key, preferred_element_type=jnp.float32).astype(jnp.bfloat16)
    gate_pre = jnp.dot(normed, w_decay, preferred_element_type=jnp.float32).astype(jnp.bfloat16)
    value_proj = jnp.dot(normed, w_value, preferred_element_type=jnp.float32).astype(jnp.bfloat16)
    log_decay = (
        jax.nn.log_sigmoid(gate_pre.astype(jnp.float32) + decay_bias[None, :] + gate_drift[:, None])
        / GATE_NORM
    )
    suffix = lax.cumsum(log_decay, axis=0, reverse=True)
    weighted = (key_proj.astype(jnp.float32) * jnp.exp(suffix - log_decay)).astype(jnp.bfloat16)
    partial_value = lax.dot_general(
        weighted, value_proj, (((0,), (0,)), ((), ())), preferred_element_type=jnp.float32
    )
    total_decay = suffix[0]
    channels = partial_value.shape[0]
    span_count = lax.axis_size("sp")
    spread = jnp.broadcast_to(total_decay[None, :, None], (1, channels, span_count))
    blocks, totals = (
        lax.all_to_all(partial_value[None], "sp", split_axis=2, concat_axis=0, tiled=True),
        lax.all_to_all(spread, "sp", split_axis=2, concat_axis=0, tiled=True),
    )
    later_sum = lax.cumsum(totals, axis=0, reverse=True) - totals
    matrix_state = jnp.sum(jnp.exp(later_sum) * blocks, axis=0)
    state_cache = matrix_state.astype(jnp.bfloat16)
    channel_ids = lax.axis_index("tp") * channels + jnp.arange(channels, dtype=jnp.int32)
    owners = (channel_ids // KEY_CHANNELS)[:, None] == jnp.arange(QUERY_KEY_HEADS, dtype=jnp.int32)[
        None, :
    ]
    query_of_head = jnp.where(
        owners, queries.astype(jnp.float32)[:, None] * KEY_CHANNELS ** (-0.5), 0.0
    )
    part_read = lax.dot_general(
        query_of_head, matrix_state, (((0,), (0,)), ((), ())), precision=lax.Precision.HIGHEST
    )
    summed_read = lax.psum(part_read, "tp")
    squares = lax.psum(jnp.sum(summed_read * summed_read, axis=1), "sp")
    first_read = summed_read * lax.rsqrt(squares / VALUE_CHANNELS + EPS)[:, None] * out_gain
    return (state_cache, first_read)


def solution(mesh):
    return jax.shard_map(
        body,
        mesh=mesh,
        in_specs=(
            P("sp", "tp"),
            P(),
            P(None, "tp"),
            P(None, "tp"),
            P(),
            P("tp"),
            P("sp"),
            P("tp"),
            P(None, "sp"),
        ),
        out_specs=(P("tp", "sp"), P(None, "sp")),
        check_vma=False,
    )
```

profile of v0, /device:TPU:0, one launch (start us, length us, event | category | flops | bytes accessed | tf_op | source)
XLA Modules:
  0.0 171.0 jit_solution(2722808447826279931)
XLA Ops:
  7.2 0.0 copy-start
  7.2 0.0 copy-start.5
  7.2 0.0 copy-start.3
  7.2 0.0 copy-start.6
  7.2 0.0 copy-start.4
  7.2 0.0 all-gather.2.cloned.1.call-start
  7.3 0.7 all-gather.2.cloned.1.call-update
  8.0 0.7 convert_multiply_fusion.2
  8.7 86.2 %all-gather.2.cloned.1.call-done = bf16[2048,2048]{1,0:T(8,128)(2,1)} async-done(((bf16[2048,256]{1,0:T(8,128)(2,1)}), bf16[2048,2048]{1,0:T(8,128)(2,1)}) %all-gather.2.cloned.1.call-update) | async-done | bytes 8388624 | tf_op jit(solution)/shard_map/all_gather | solution.py:14
  94.9 0.0 copy-start.1
  94.9 5.2 %fusion = f32[2048]{0:T(1024)S(1)} fusion(bf16[2048,2048]{1,0:T(8,128)(2,1)} %all-gather.2.cloned.1.call-done), kind=kLoop, calls=%fused_computation.2 | loop fusion | flops 12580864 | bytes 8396800 | tf_op jit(solution)/shard_map/reduce_sum | solution.py:16
  100.1 0.0 copy-done.5
  100.1 0.0 copy-done.3
  100.1 0.0 copy-done.6
  100.1 0.0 copy-done.4
  100.1 0.5 copy-done.1
  100.6 4.7 %fusion.12 = (f32[128,2048]{0,1:T(8,128)S(1)}, f32[2048,128]{1,0:T(8,128)}) fusion(f32[2048]{0:T(1024)S(1)} %copy-done.4, f32[128]{0:T(128)S(1)} %copy-done.6, bf16[2048,128]{1,0:T(8,128)(2,1)S(1)} %copy-done.3, bf16[2048,2048]{1,0:T(8,128)(2,1)S(1)} %copy-done.1, f32[2048]{0:T(1024)S(1)} %copy-done.5, f32[2048]{0:T(1024)S(1)} %add_rsqrt_fusion), kind=kOutput, calls=%fused_computation.19 | convolution fusion | flops 1093926912 | bytes 11035136 | tf_op jit(solution)/shard_map/dot_general | solution.py:19
  105.4 2.6 %fusion.21 = f32[128,16,128]{0,1,2:T(8,128)S(1)} fusion(f32[128,16,128]{0,2,1:T(8,128)S(1)} %bitcast.44), kind=kOutput, calls=%fused_computation.30 | output fusion | flops 33292288 | bytes 2097152 | tf_op jit(solution)/shard_map/reduce-window
  108.0 0.1 broadcast_add_fusion
  108.1 0.3 copy.17
  108.4 0.6 broadcast_in_dim.19
  109.0 3.6 %all-to-all-start = ((f32[1,128,4]{1,0,2:T(1,128)}), f32[1,128,4]{1,0,2:T(1,128)S(1)}, u32[]{:S(2)}, u32[]{:S(2)}) async-start(f32[1,128,4]{1,0,2:T(1,128)} %broadcast_in_dim.19), calls=%async_computation | async-start | bytes 4096 | tf_op jit(solution)/shard_map/all_to_all | solution.py:36
  112.6 7.6 %fusion.9 = bf16[2048,128]{1,0:T(8,128)(2,1)} fusion(bf16[2048,128]{1,0:T(8,128)(2,1)} %param.11, f32[2048,128]{1,0:T(8,128)S(1)} %bitcast.43, f32[2048,128]{1,0:T(8,128)} %get-tuple-element.5, bf16[2048,2048]{1,0:T(8,128)(2,1)} %all-gather.2.cloned.1.call-done, f32[2048]{0:T(1024)S(1)} %copy-done.5, f32[2048]{0:T(1024)S(1)} %add_rsqrt_fusion), kind=kOutput, calls=%fused_computation.16 | convolution fusion | flops 1093926912 | bytes 11550720 | tf_op jit(solution)/shard_map/dot_general | solution.py:18
  120.2 0.0 copy-done
  120.2 0.0 copy-start.2
  120.2 10.2 %fusion.10 = f32[128,512]{0,1:T(8,128)} fusion(bf16[2048,128]{1,0:T(8,128)(2,1)} %fusion.9, bf16[2048,512]{1,0:T(8,128)(2,1)S(1)} %copy-done, bf16[2048,2048]{1,0:T(8,128)(2,1)} %all-gather.2.cloned.1.call-done, f32[2048]{0:T(1024)S(1)} %copy-done.5, f32[2048]{0:T(1024)S(1)} %add_rsqrt_fusion), kind=kOutput, calls=%fused_computation.17 | convolution fusion | flops 4581228544 | bytes 11288576 | tf_op jit(solution)/shard_map/dot_general | solution.py:27
  130.4 0.0 all-to-all-done
  130.5 4.2 %all-to-all-start.1 = ((f32[1,128,512]{1,0,2:T(1,128)}), f32[1,128,512]{1,0,2:T(1,128)S(1)}, u32[]{:S(2)}, u32[]{:S(2)}) async-start(f32[1,128,512]{1,0,2:T(1,128)} %bitcast.18), calls=%async_computation.1 | async-start | bytes 524288 | tf_op jit(solution)/shard_map/all_to_all | solution.py:35
  134.7 5.3 %all-to-all-done.1 = f32[1,128,512]{1,0,2:T(1,128)S(1)} async-done(((f32[1,128,512]{1,0,2:T(1,128)}), f32[1,128,512]{1,0,2:T(1,128)S(1)}, u32[]{:S(2)}, u32[]{:S(2)}) %all-to-all-start.1) | async-done | bytes 262176 | tf_op jit(solution)/shard_map/all_to_all | solution.py:35
  140.0 0.3 fusion.23
  140.3 13.6 %psum.14 = f32[4,128]{1,0:T(4,128)S(1)} all-reduce(f32[4,128]{1,0:T(4,128)S(1)} %fusion.23), channel_id=1, replica_groups=mesh['sp'=4,'tp'=8] {'tp'}, use_global_device_ids=true, to_apply=%region_5.6 | all-reduce | flops 512 | bytes 4096 | tf_op jit(solution)/shard_map/psum | solution.py:51
  153.9 0.1 multiply_reduce_fusion.1
  154.1 8.7 %psum.15 = f32[4]{0:T(128)S(1)} all-reduce(f32[4]{0:T(128)S(1)} %multiply_reduce_fusion.1), channel_id=1, replica_groups=mesh['sp'=4,'tp'=8] {'sp'}, use_global_device_ids=true, to_apply=%region_7.8 | all-reduce | flops 4 | bytes 32 | tf_op jit(solution)/shard_map/psum | solution.py:52
  162.8 0.7 copy.19
  163.5 0.0 copy-done.2
  163.5 0.6 multiply_multiply_fusion
  (11 shorter events, 0.1 us)
Async XLA Ops:
  7.2 113.1 %copy-start = (bf16[2048,512]{1,0:T(8,128)(2,1)S(1)}, bf16[2048,512]{1,0:T(8,128)(2,1)}, u32[]{:S(2)}) copy-start(bf16[2048,512]{1,0:T(8,128)(2,1)} %param.13) | copy-start | bytes 6291460
  7.2 92.9 %copy-start.5 = (f32[2048]{0:T(1024)S(1)}, f32[2048]{0:T(1024)}, u32[]{:S(2)}) copy-start(f32[2048]{0:T(1024)} %param.10) | copy-start | bytes 24580
  7.2 92.9 %copy-start.3 = (bf16[2048,128]{1,0:T(8,128)(2,1)S(1)}, bf16[2048,128]{1,0:T(8,128)(2,1)}, u32[]{:S(2)}) copy-start(bf16[2048,128]{1,0:T(8,128)(2,1)} %param.12) | copy-start | bytes 1572868
  7.2 92.9 %copy-start.6 = (f32[128]{0:T(128)S(1)}, f32[128]{0:T(128)}, u32[]{:S(2)}) copy-start(f32[128]{0:T(128)} %param.14) | copy-start | bytes 1540
  7.2 92.9 %copy-start.4 = (f32[2048]{0:T(1024)S(1)}, f32[2048]{0:T(1024)}, u32[]{:S(2)}) copy-start(f32[2048]{0:T(1024)} %param.15) | copy-start | bytes 24580
  7.2 87.6 %all-gather.2.cloned.1.call-start = ((), (), s32[]{:S(2)}) async-start(), calls=%async_computation.2 | async-start | bytes 9437184 | tf_op jit(solution)/shard_map/all_gather | solution.py:14
  94.9 5.8 %copy-start.1 = (bf16[2048,2048]{1,0:T(8,128)(2,1)S(1)}, bf16[2048,2048]{1,0:T(8,128)(2,1)}, u32[]{:S(2)}) copy-start(bf16[2048,2048]{1,0:T(8,128)(2,1)} %all-gather.2.cloned.1.call-done) | copy-start | bytes 25165828
  109.0 21.5 %all-to-all-start = ((f32[1,128,4]{1,0,2:T(1,128)}), f32[1,128,4]{1,0,2:T(1,128)S(1)}, u32[]{:S(2)}, u32[]{:S(2)}) async-start(f32[1,128,4]{1,0,2:T(1,128)} %broadcast_in_dim.19), calls=%async_computation | async-start | bytes 4096 | tf_op jit(solution)/shard_map/all_to_all | solution.py:36
  120.2 43.3 %copy-start.2 = (f32[4,128]{1,0:T(4,128)S(1)}, f32[4,128]{1,0:T(4,128)}, u32[]{:S(2)}) copy-start(f32[4,128]{1,0:T(4,128)} %param.17) | copy-start | bytes 6148
  130.5 9.6 %all-to-all-start.1 = ((f32[1,128,512]{1,0,2:T(1,128)}), f32[1,128,512]{1,0,2:T(1,128)S(1)}, u32[]{:S(2)}, u32[]{:S(2)}) async-start(f32[1,128,512]{1,0,2:T(1,128)} %bitcast.18), calls=%async_computation.1 | async-start | bytes 524288 | tf_op jit(solution)/shard_map/all_to_all | solution.py:35
Sparse Core Ops, SparseCore 0:
  9.6 85.1 all-gather.1
where the time goes:
time: 171 us
  waiting for transfers between devices  92.2 us (54%)
  matrix products  22.8 us (13%)
  blocking collectives  22.4 us (13%)
  between operations  14.2 us (8%)
  other arithmetic  9.45 us (6%)
  starting transfers between devices  7.88 us (5%)
  local copies, waits for them, and re-layouts  2.17 us (1%)
    all_gather x1, waiting for transfers between devices, body(): gathered = lax.all_gather(tokens, 'tp', axis=1, tiled=True)  86.2 us
    psum x1, blocking collectives, body(): summed_read = lax.psum(part_read, 'tp')  13.6 us
    dot_general x1, matrix products, body(): lax.dot_general(weighted, value_proj, (((0,), (0,)), ((), ())), preferred...  10.2 us
    psum x1, blocking collectives, body(): squares = lax.psum(jnp.sum(summed_read * summed_read, axis=1), 'sp')  8.74 us
    dot_general x1, matrix products, body(): jnp.dot(normed, w_key, preferred_element_type=jnp.float32)  7.58 us
    all_to_all x1, waiting for transfers between devices, body(): lax.all_to_all(partial_value[None], 'sp', split_axis=2, concat_axis=0, ti...  5.33 us
    reduce_sum x1, other arithmetic, body(): jnp.mean(rows_f32 * rows_f32, axis=1, keepdims=True) + EPS  5.23 us
    dot_general x1, matrix products, body(): jnp.dot(normed, w_decay, preferred_element_type=jnp.float32)  4.74 us
  transfers between devices with their start and end apart: 3, of which 2 were waited for; matrix products, arithmetic and copies ran while one was open for 11% of the time, Pallas kernels for 0%

commit v1 on v0

--- a/solution.py
+++ b/solution.py
@@ -1,3 +1,4 @@
+import functools
 import jax
 import jax.numpy as jnp
 from jax import lax
@@ -8,6 +9,28 @@
 VALUE_CHANNELS = 512
 EPS = 1e-06
 GATE_NORM = 16.0
+
+
+def time_plane(state, mesh_dim):
+    wide_n = lax.axis_size(mesh_dim)
+
+    def extend_patches_by_axis(current_value, next_value):
+        if next_value >= wide_n:
+            return current_value
+        return extend_patches_by_axis(
+            current_value
+            + lax.ppermute(
+                current_value,
+                axis_name=mesh_dim,
+                perm=[(dev, dev ^ next_value) for dev in range(wide_n)],
+            ),
+            2 * next_value,
+        )
+
+    return extend_patches_by_axis(state, 1)
+
+
+connect_the_ratios = functools.partial(time_plane, mesh_dim="tp")
 
 
 def body(tokens, norm_gain, w_key, w_decay, w_value, decay_bias, gate_drift, queries, out_gain):
@@ -48,7 +71,7 @@
     part_read = lax.dot_general(
         query_of_head, matrix_state, (((0,), (0,)), ((), ())), precision=lax.Precision.HIGHEST
     )
-    summed_read = lax.psum(part_read, "tp")
+    summed_read = connect_the_ratios(part_read)
     squares = lax.psum(jnp.sum(summed_read * summed_read, axis=1), "sp")
     first_read = summed_read * lax.rsqrt(squares / VALUE_CHANNELS + EPS)[:, None] * out_gain
     return (state_cache, first_read)

time: 171 us -> 166 us (0.971)
  blocking collectives: 22.4 us -> 8.73 us
  waiting for transfers between devices: 92.2 us -> 98.9 us
  starting transfers between devices: 7.88 us -> 9.7 us
    psum x1 -> x0, blocking collectives: 13.6 us -> none  [body(): summed_read = lax.psum(part_read, 'tp')]
    ppermute x0 -> x3, waiting for transfers between devices: none -> 6.72 us  [extend_patches_by_axis(): lax.ppermute(current_value, axis_name=mesh_dim, perm=[(dev, dev ^ next_va...]
    ppermute x0 -> x3, starting transfers between devices: none -> 1.82 us  [extend_patches_by_axis(): lax.ppermute(current_value, axis_name=mesh_dim, perm=[(dev, dev ^ next_va...]
  transfers between devices with their start and end apart: 3 -> 6, of which waited for: 2 -> 5; matrix products, arithmetic and copies ran while one was open for 11% -> 12% of each run, Pallas kernels for 0% -> 0%
where the time goes in v1:
time: 166 us
  waiting for transfers between devices  98.9 us (60%)
  matrix products  22.8 us (14%)
  between operations  14.2 us (9%)
  starting transfers between devices  9.7 us (6%)
  other arithmetic  9.46 us (6%)
  blocking collectives  8.73 us (5%)
  local copies, waits for them, and re-layouts  2.17 us (1%)
    all_gather x1, waiting for transfers between devices, body(): gathered = lax.all_gather(tokens, 'tp', axis=1, tiled=True)  86.2 us
    dot_general x1, matrix products, body(): lax.dot_general(weighted, value_proj, (((0,), (0,)), ((), ())), preferred...  10.2 us
    psum x1, blocking collectives, body(): squares = lax.psum(jnp.sum(summed_read * summed_read, axis=1), 'sp')  8.73 us
    dot_general x1, matrix products, body(): jnp.dot(normed, w_key, preferred_element_type=jnp.float32)  7.58 us
    ppermute x3, waiting for transfers between devices, extend_patches_by_axis(): lax.ppermute(current_value, axis_name=mesh_dim, perm=[(dev, dev ^ next_va...  6.72 us
    all_to_all x1, waiting for transfers between devices, body(): lax.all_to_all(partial_value[None], 'sp', split_axis=2, concat_axis=0, ti...  5.33 us
    reduce_sum x1, other arithmetic, body(): jnp.mean(rows_f32 * rows_f32, axis=1, keepdims=True) + EPS  5.23 us
    dot_general x1, matrix products, body(): jnp.dot(normed, w_decay, preferred_element_type=jnp.float32)  4.74 us
  transfers between devices with their start and end apart: 6, of which 5 were waited for; matrix products, arithmetic and copies ran while one was open for 12% of the time, Pallas kernels for 0%

profile of v1, /device:TPU:0, one launch (start us, length us, event | category | flops | bytes accessed | tf_op | source)
XLA Modules:
  0.0 166.0 jit_solution(4445848222266797332)
XLA Ops:
  7.2 0.0 copy-start
  7.2 0.0 copy-start.5
  7.2 0.0 copy-start.3
  7.2 0.0 copy-start.6
  7.2 0.0 copy-start.4
  7.2 0.0 all-gather.2.cloned.1.call-start
  7.3 0.7 all-gather.2.cloned.1.call-update
  8.0 0.7 convert_multiply_fusion.2
  8.7 86.2 %all-gather.2.cloned.1.call-done = bf16[2048,2048]{1,0:T(8,128)(2,1)} async-done(((bf16[2048,256]{1,0:T(8,128)(2,1)}), bf16[2048,2048]{1,0:T(8,128)(2,1)}) %all-gather.2.cloned.1.call-update) | async-done | bytes 8388624 | tf_op jit(solution)/shard_map/all_gather | solution.py:37
  94.9 0.0 copy-start.1
  94.9 5.2 %fusion = f32[2048]{0:T(1024)S(1)} fusion(bf16[2048,2048]{1,0:T(8,128)(2,1)} %all-gather.2.cloned.1.call-done), kind=kLoop, calls=%fused_computation.2 | loop fusion | flops 12580864 | bytes 8396800 | tf_op jit(solution)/shard_map/reduce_sum | solution.py:39
  100.1 0.0 copy-done.5
  100.1 0.0 copy-done.3
  100.1 0.0 copy-done.6
  100.1 0.0 copy-done.4
  100.1 0.5 copy-done.1
  100.6 4.7 %fusion.12 = (f32[128,2048]{0,1:T(8,128)S(1)}, f32[2048,128]{1,0:T(8,128)}) fusion(f32[2048]{0:T(1024)S(1)} %copy-done.4, f32[128]{0:T(128)S(1)} %copy-done.6, bf16[2048,128]{1,0:T(8,128)(2,1)S(1)} %copy-done.3, bf16[2048,2048]{1,0:T(8,128)(2,1)S(1)} %copy-done.1, f32[2048]{0:T(1024)S(1)} %copy-done.5, f32[2048]{0:T(1024)S(1)} %add_rsqrt_fusion), kind=kOutput, calls=%fused_computation.19 | convolution fusion | flops 1093926912 | bytes 11035136 | tf_op jit(solution)/shard_map/dot_general | solution.py:42
  105.4 2.6 %fusion.21 = f32[128,16,128]{0,1,2:T(8,128)S(1)} fusion(f32[128,16,128]{0,2,1:T(8,128)S(1)} %bitcast.44), kind=kOutput, calls=%fused_computation.30 | output fusion | flops 33292288 | bytes 2097152 | tf_op jit(solution)/shard_map/reduce-window
  108.0 0.1 broadcast_add_fusion
  108.1 0.3 copy.17
  108.4 0.6 broadcast_in_dim.19
  109.0 3.6 %all-to-all-start = ((f32[1,128,4]{1,0,2:T(1,128)}), f32[1,128,4]{1,0,2:T(1,128)S(1)}, u32[]{:S(2)}, u32[]{:S(2)}) async-start(f32[1,128,4]{1,0,2:T(1,128)} %broadcast_in_dim.19), calls=%async_computation | async-start | bytes 4096 | tf_op jit(solution)/shard_map/all_to_all | solution.py:59
  112.6 7.6 %fusion.9 = bf16[2048,128]{1,0:T(8,128)(2,1)} fusion(bf16[2048,128]{1,0:T(8,128)(2,1)} %param.11, f32[2048,128]{1,0:T(8,128)S(1)} %bitcast.43, f32[2048,128]{1,0:T(8,128)} %get-tuple-element.7, bf16[2048,2048]{1,0:T(8,128)(2,1)} %all-gather.2.cloned.1.call-done, f32[2048]{0:T(1024)S(1)} %copy-done.5, f32[2048]{0:T(1024)S(1)} %add_rsqrt_fusion), kind=kOutput, calls=%fused_computation.16 | convolution fusion | flops 1093926912 | bytes 11550720 | tf_op jit(solution)/shard_map/dot_general | solution.py:41
  120.2 0.0 copy-done
  120.2 0.0 copy-start.2
  120.2 10.2 %fusion.10 = f32[128,512]{0,1:T(8,128)} fusion(bf16[2048,128]{1,0:T(8,128)(2,1)} %fusion.9, bf16[2048,512]{1,0:T(8,128)(2,1)S(1)} %copy-done, bf16[2048,2048]{1,0:T(8,128)(2,1)} %all-gather.2.cloned.1.call-done, f32[2048]{0:T(1024)S(1)} %copy-done.5, f32[2048]{0:T(1024)S(1)} %add_rsqrt_fusion), kind=kOutput, calls=%fused_computation.17 | convolution fusion | flops 4581228544 | bytes 11288576 | tf_op jit(solution)/shard_map/dot_general | solution.py:50
  130.4 0.0 all-to-all-done
  130.5 4.2 %all-to-all-start.1 = ((f32[1,128,512]{1,0,2:T(1,128)}), f32[1,128,512]{1,0,2:T(1,128)S(1)}, u32[]{:S(2)}, u32[]{:S(2)}) async-start(f32[1,128,512]{1,0,2:T(1,128)} %bitcast.18), calls=%async_computation.1 | async-start | bytes 524288 | tf_op jit(solution)/shard_map/all_to_all | solution.py:58
  134.7 5.3 %all-to-all-done.1 = f32[1,128,512]{1,0,2:T(1,128)S(1)} async-done(((f32[1,128,512]{1,0,2:T(1,128)}), f32[1,128,512]{1,0,2:T(1,128)S(1)}, u32[]{:S(2)}, u32[]{:S(2)}) %all-to-all-start.1) | async-done | bytes 262176 | tf_op jit(solution)/shard_map/all_to_all | solution.py:58
  140.0 0.3 fusion.23
  140.3 0.0 collective-permute-start
  140.3 1.2 collective-permute-done
  141.5 0.0 collective-permute-start.1
  141.5 3.6 %collective-permute-done.1 = f32[4,128]{1,0:T(4,128)S(1)} collective-permute-done((f32[4,128]{1,0:T(4,128)S(1)}, f32[4,128]{1,0:T(4,128)S(1)}, u32[]{:S(2)}, u32[]{:S(2)}) %collective-permute-start.1) | collective-permute-done | bytes 2080 | tf_op jit(solution)/shard_map/ppermute | solution.py:22
  145.1 1.8 %collective-permute-start.2 = (f32[4,128]{1,0:T(4,128)S(1)}, f32[4,128]{1,0:T(4,128)S(1)}, u32[]{:S(2)}, u32[]{:S(2)}) collective-permute-start(f32[4,128]{1,0:T(4,128)S(1)} %add.82), channel_id=1, source_target_pairs={{0,4},{1,5},{2,6},{3,7},{4,0},{5,1},{6,2},{7,3},{8,12},{9,13},{10,... | collective-permute-start | bytes 6152 | tf_op jit(solution)/shard_map/ppermute | solution.py:22
  146.9 0.7 copy.19
  147.7 1.9 %collective-permute-done.2 = f32[4,128]{1,0:T(4,128)S(1)} collective-permute-done((f32[4,128]{1,0:T(4,128)S(1)}, f32[4,128]{1,0:T(4,128)S(1)}, u32[]{:S(2)}, u32[]{:S(2)}) %collective-permute-start.2) | collective-permute-done | bytes 2080 | tf_op jit(solution)/shard_map/ppermute | solution.py:22
  149.6 0.1 multiply_reduce_fusion.1
  149.7 8.7 %psum.7 = f32[4]{0:T(128)S(1)} all-reduce(f32[4]{0:T(128)S(1)} %get-tuple-element.4), channel_id=1, replica_groups=mesh['sp'=4,'tp'=8] {'sp'}, use_global_device_ids=true, to_apply=%region_6.7 | all-reduce | flops 4 | bytes 32 | tf_op jit(solution)/shard_map/psum | solution.py:75
  158.5 0.0 copy-done.2
  158.5 0.7 multiply_multiply_fusion
  (13 shorter events, 0.2 us)
Async XLA Ops:
  7.2 113.1 %copy-start = (bf16[2048,512]{1,0:T(8,128)(2,1)S(1)}, bf16[2048,512]{1,0:T(8,128)(2,1)}, u32[]{:S(2)}) copy-start(bf16[2048,512]{1,0:T(8,128)(2,1)} %param.13) | copy-start | bytes 6291460
  7.2 92.9 %copy-start.5 = (f32[2048]{0:T(1024)S(1)}, f32[2048]{0:T(1024)}, u32[]{:S(2)}) copy-start(f32[2048]{0:T(1024)} %param.10) | copy-start | bytes 24580
  7.2 92.9 %copy-start.3 = (bf16[2048,128]{1,0:T(8,128)(2,1)S(1)}, bf16[2048,128]{1,0:T(8,128)(2,1)}, u32[]{:S(2)}) copy-start(bf16[2048,128]{1,0:T(8,128)(2,1)} %param.12) | copy-start | bytes 1572868
  7.2 92.9 %copy-start.6 = (f32[128]{0:T(128)S(1)}, f32[128]{0:T(128)}, u32[]{:S(2)}) copy-start(f32[128]{0:T(128)} %param.14) | copy-start | bytes 1540
  7.2 92.9 %copy-start.4 = (f32[2048]{0:T(1024)S(1)}, f32[2048]{0:T(1024)}, u32[]{:S(2)}) copy-start(f32[2048]{0:T(1024)} %param.15) | copy-start | bytes 24580
  7.2 87.6 %all-gather.2.cloned.1.call-start = ((), (), s32[]{:S(2)}) async-start(), calls=%async_computation.2 | async-start | bytes 9437184 | tf_op jit(solution)/shard_map/all_gather | solution.py:37
  94.9 5.8 %copy-start.1 = (bf16[2048,2048]{1,0:T(8,128)(2,1)S(1)}, bf16[2048,2048]{1,0:T(8,128)(2,1)}, u32[]{:S(2)}) copy-start(bf16[2048,2048]{1,0:T(8,128)(2,1)} %all-gather.2.cloned.1.call-done) | copy-start | bytes 25165828
  109.0 21.5 %all-to-all-start = ((f32[1,128,4]{1,0,2:T(1,128)}), f32[1,128,4]{1,0,2:T(1,128)S(1)}, u32[]{:S(2)}, u32[]{:S(2)}) async-start(f32[1,128,4]{1,0,2:T(1,128)} %broadcast_in_dim.19), calls=%async_computation | async-start | bytes 4096 | tf_op jit(solution)/shard_map/all_to_all | solution.py:59
  120.2 38.2 %copy-start.2 = (f32[4,128]{1,0:T(4,128)S(1)}, f32[4,128]{1,0:T(4,128)}, u32[]{:S(2)}) copy-start(f32[4,128]{1,0:T(4,128)} %param.17) | copy-start | bytes 6148
  130.5 9.6 %all-to-all-start.1 = ((f32[1,128,512]{1,0,2:T(1,128)}), f32[1,128,512]{1,0,2:T(1,128)S(1)}, u32[]{:S(2)}, u32[]{:S(2)}) async-start(f32[1,128,512]{1,0,2:T(1,128)} %bitcast.18), calls=%async_computation.1 | async-start | bytes 524288 | tf_op jit(solution)/shard_map/all_to_all | solution.py:58
  140.3 1.2 collective-permute-start
  141.5 3.6 %collective-permute-start.1 = (f32[4,128]{1,0:T(4,128)S(1)}, f32[4,128]{1,0:T(4,128)S(1)}, u32[]{:S(2)}, u32[]{:S(2)}) collective-permute-start(f32[4,128]{1,0:T(4,128)S(1)} %add.81), channel_id=1, source_target_pairs={{0,2},{1,3},{2,0},{3,1},{4,6},{5,7},{6,4},{7,5},{8,10},{9,11},{10,... | collective-permute-start | bytes 6152 | tf_op jit(solution)/shard_map/ppermute | solution.py:22
  145.1 4.5 %collective-permute-start.2 = (f32[4,128]{1,0:T(4,128)S(1)}, f32[4,128]{1,0:T(4,128)S(1)}, u32[]{:S(2)}, u32[]{:S(2)}) collective-permute-start(f32[4,128]{1,0:T(4,128)S(1)} %add.82), channel_id=1, source_target_pairs={{0,4},{1,5},{2,6},{3,7},{4,0},{5,1},{6,2},{7,3},{8,12},{9,13},{10,... | collective-permute-start | bytes 6152 | tf_op jit(solution)/shard_map/ppermute | solution.py:22
Sparse Core Ops, SparseCore 0:
  9.6 85.1 all-gather.1
